TPU v7x, 32 devices: a whole 2x2x4 slice. The times are simulated.
32 devices in a mesh: fs: 8 (over z, y), tp: 4 (over x, core).
Axes of the slice: x: 2, y: 2, z: 4, core: 2. Of those that a mesh axis runs over, the one named last changes fastest.
Arguments:
- mixed: bfloat16 [12288, 2048], P(('fs', 'tp')), may hold values from -6 to 6
- residual: bfloat16 [12288, 2048], P(('fs', 'tp')), may hold values from -6 to 6
- mix_weight: bfloat16 [2048, 2048], P(('fs', 'tp')), may hold values from -0.125 to 0.125
- norm_gain: float32 [2048], replicated, may hold values from 0.1 to 1.9
- up_weight: bfloat16 [2048, 5504], P('fs', 'tp'), may hold values from -0.125 to 0.125
- gate_weight: bfloat16 [2048, 5504], P('fs', 'tp'), may hold values from -0.125 to 0.125
- conv_weight: float32 [3, 5504], P(None, 'tp'), may hold values from -3 to 3
- conv_bias: float32 [5504], P('tp'), may hold values from -3 to 3
- down_weight: bfloat16 [5504, 2048], P('tp', 'fs'), may hold values from -0.078125 to 0.078125
Outputs:
- output: bfloat16 [12288, 2048], P(('fs', 'tp'))
All inputs are finite; a program needn't handle non-finite values.
Results may differ from a plain program's by a relative error of at most 0.012.
Values may be sent and summed in bfloat16 or wider, within the bound.
A program may use at most 128 MiB of HBM per device.

v0:
```python
import functools

import jax
import jax.numpy as jnp
from jax import lax
from jax.experimental import pallas as pl
from jax.experimental.pallas import tpu as pltpu
from jax.sharding import PartitionSpec as P


norm_eps = 1e-06
f32, bf16 = jnp.float32, jnp.bfloat16
MESH = pl.DeviceIdType.MESH


def gather_kernel(nz, ny, nx, plan, count, spread, *refs):
    shards, fulls = refs[:count], refs[count : 2 * count]
    send_sem, recv_sem, local_sem, tp_send, tp_recv = refs[2 * count :]
    n_fs = nz * ny
    me = lax.axis_index("fs")
    z, y = me // ny, lax.rem(me, ny)
    tp = lax.axis_index("tp")
    x, core = tp // 2, lax.rem(tp, 2)

    def x_at(dx):
        return lax.rem(x + dx, nx) * 2 + core

    def fs_at(zz, dy):
        return zz * ny + lax.rem(y + dy, ny)

    def part(f, t):
        rows = plan[0][4]
        return fulls[0].at[pl.ds(pl.multiple_of((f * (2 * nx) + t) * rows, 16), rows), :]

    def piece(c, f):
        m, axis, block, off, size, _ = plan[c]
        if spread and c == 0:
            return part(f, tp)
        if axis == 0:
            return fulls[m].at[pl.ds(pl.multiple_of(f * block + off, 16), size), :]
        return fulls[m].at[:, pl.ds(pl.multiple_of(f * block + off, 128), size)]

    def own(c):
        m, axis, _, off, size, _ = plan[c]
        return shards[m].at[off : off + size, :] if axis == 0 else shards[m].at[:, off : off + size]

    def copy(c, f, lane, to, mine=False):
        return pltpu.make_async_remote_copy(
            src_ref=own(c) if mine else piece(c, f),
            dst_ref=piece(c, f),
            send_sem=send_sem.at[lane, f, c],
            recv_sem=recv_sem.at[f, c],
            device_id={"fs": to},
            device_id_type=MESH,
        )

    def arrived(c, f):
        copy(c, f, 0, lax.rem(me + 1, n_fs)).wait_recv()

    def z_sends(act, c, f, up, down, mine=False):
        if up:

            @pl.when(z < nz - 1)
            def _():
                act(copy(c, f, 0, me + ny, mine))

        if down:

            @pl.when(z > 0)
            def _():
                act(copy(c, f, 1, me - ny, mine))

    def y_sends(act, c, f, mine=False):
        for dy in range(1, ny):
            act(copy(c, f, 1 + dy, fs_at(z, dy), mine))

    def tp_copy(f, t, lane, to):
        return pltpu.make_async_remote_copy(
            src_ref=part(f, t),
            dst_ref=part(f, t),
            send_sem=tp_send.at[f, lane],
            recv_sem=tp_recv.at[f, t],
            device_id={"tp": to},
            device_id_type=MESH,
        )

    def tp_sends(act, f):
        for dx in range(1, nx):
            act(tp_copy(f, tp, dx - 1, x_at(dx)))
        act(tp_copy(f, tp, nx - 1, tp + 1 - 2 * core))

    def tp_relay(act, f, wait):
        for dx in range(1, nx):
            if wait:
                tp_copy(f, x_at(dx), 0, x_at(dx)).wait_recv()
            act(tp_copy(f, x_at(dx), nx - 1 + dx, tp + 1 - 2 * core))

    def local(c):
        return pltpu.make_async_copy(own(c), piece(c, me), local_sem.at[c])

    barrier = pltpu.get_barrier_semaphore()
    greet = [lax.rem(me + ny, n_fs), lax.rem(me + n_fs - ny, n_fs)]
    greet += [fs_at(z, dy) for dy in range(1, ny)]
    for other in greet:
        pl.semaphore_signal(barrier, inc=1, device_id={"fs": other}, device_id_type=MESH)
    greet_tp = [x_at(dx) for dx in range(1, nx)] + [tp + 1 - 2 * core] if spread else []
    for other in greet_tp:
        pl.semaphore_signal(barrier, inc=1, device_id={"tp": other}, device_id_type=MESH)
    pl.semaphore_wait(barrier, len(greet) + len(greet_tp))

    def walk(act, wait):
        for c in range(len(plan)):
            y_sends(act, c, me, True)
            z_sends(act, c, me, True, True, True)
        if wait:
            for c in range(len(plan)):
                local(c).start()
        if spread:
            if wait:
                local(0).wait()
            tp_sends(act, me)
        for c in range(len(plan)):
            if plan[c][5]:
                for dy in range(1, ny):
                    f = fs_at(z, dy)
                    if wait:
                        arrived(c, f)
                    z_sends(act, c, f, True, True)

        def from_y(zz):
            for dy in range(1, ny):
                f = fs_at(zz, dy)
                if wait:
                    arrived(0, f)
                tp_sends(act, f)

        def both(t, do):
            for below in (True, False) if t else (True,):
                zz = z - t if below else z + t
                pl.when(zz >= 0 if below else zz < nz)(functools.partial(do, zz))

        for t in range(1, nz):
            if spread:
                both(t - 1, from_y)
            for c in range(len(plan)):
                for below in (True, False):
                    zz = z - t if below else z + t

                    @pl.when(zz >= 0 if below else zz < nz)
                    def _():
                        for dy in range(ny) if plan[c][5] else (0,):
                            f = fs_at(zz, dy)
                            if wait:
                                arrived(c, f)
                            z_sends(act, c, f, below, not below)
                            if not plan[c][5]:
                                y_sends(act, c, f)
                            if spread and c == 0:
                                tp_sends(act, f)

        if spread:
            both(nz - 1, from_y)
            for f in range(n_fs):
                tp_relay(act, f, wait)

    walk(lambda d: d.start(), True)
    if spread:
        for f in range(n_fs):
            for dx in range(nx):
                t = x_at(dx) + 1 - 2 * core
                tp_copy(f, t, 0, tp + 1 - 2 * core).wait_recv()
    for c in range(1 if spread else 0, len(plan)):
        if not plan[c][5]:
            for zz in range(nz):
                for dy in range(1, ny):
                    arrived(c, fs_at(zz, dy))
    for c in range(1 if spread else 0, len(plan)):
        local(c).wait()
    walk(lambda d: d.wait_send(), False)


def fs_gather(shards, axes, chunks, y_first, nz, ny, nx, spread, ident):
    n_fs = nz * ny
    plan, shapes = [], []
    for m, (w, axis) in enumerate(zip(shards, axes)):
        block = w.shape[axis]
        size = max(128, block // chunks)
        size = size if block % size == 0 else block
        for off in range(0, block, size):
            plan.append((m, axis, block, off, size, len(plan) in y_first and block > size))
        shape = list(w.shape)
        shape[axis] = block * n_fs * (2 * nx if spread and m == 0 else 1)
        shapes.append(jax.ShapeDtypeStruct(tuple(shape), w.dtype))
    n = len(plan)
    return pl.pallas_call(
        functools.partial(gather_kernel, nz, ny, nx, tuple(plan), len(shards), spread),
        out_shape=shapes,
        in_specs=[pl.BlockSpec(memory_space=pl.ANY)] * len(shards),
        out_specs=[pl.BlockSpec(memory_space=pl.ANY)] * len(shards),
        scratch_shapes=[
            pltpu.SemaphoreType.DMA((1 + ny, n_fs, n)),
            pltpu.SemaphoreType.DMA((n_fs, n)),
            pltpu.SemaphoreType.DMA((n,)),
            pltpu.SemaphoreType.DMA((n_fs, 2 * nx - 1)),
            pltpu.SemaphoreType.DMA((n_fs, 2 * nx)),
        ],
        compiler_params=pltpu.CompilerParams(collective_id=ident, has_side_effects=True),
        cost_estimate=pl.CostEstimate(flops=10**11, bytes_accessed=10**7, transcendentals=0),
    )(*shards)


def make_body(n_fs, n_tp, ny):
    nz, nx = n_fs // ny, n_tp // 2

    def hop_x(a, dx):
        return lax.ppermute(
            a, "tp", [(x * 2 + c, (x + dx) % nx * 2 + c) for x in range(nx) for c in range(2)]
        )

    def hop_core(a):
        return lax.ppermute(a, "tp", [(t, t ^ 1) for t in range(n_tp)])

    def body(
        mixed,
        residual,
        mix_weight,
        norm_gain,
        up_weight,
        gate_weight,
        conv_weight,
        conv_bias,
        down_weight,
    ):
        tp_i = lax.axis_index("tp")
        core, x_i = tp_i % 2, tp_i // 2
        tok, width = residual.shape
        mix_full, up_full, gate_full = fs_gather(
            (mix_weight, up_weight, gate_weight), (0, 0, 0), 2, (1,), nz, ny, nx, True, 0
        )
        summed = jnp.dot(mixed, mix_full, preferred_element_type=f32)
        stream = (residual.astype(f32) + summed).astype(bf16)
        x_float = stream.astype(f32)
        normed = (
            x_float
            * lax.rsqrt(jnp.mean(x_float * x_float, axis=-1, keepdims=True) + norm_eps)
            * norm_gain
        ).astype(bf16)
        normed, down_weight = lax.optimization_barrier((normed, down_weight))
        tokens = lax.all_gather(normed, "tp", axis=0, tiled=True)
        (down_full,) = fs_gather((down_weight,), (1,), 2, (), nz, ny, nx, False, 1)
        tokens, down_full = lax.optimization_barrier((tokens, down_full))
        lead = 16
        tokens = jnp.pad(tokens, ((lead, 0), (0, 0)))
        total, gate_tie = x_float, up_full
        for dx in list(range(1, nx)) + [0]:
            first = (x_i + dx) % nx * 2 * tok
            rows = lax.dynamic_slice_in_dim(tokens, first, 2 * tok + lead, axis=0)
            up_part = jnp.dot(rows, gate_tie, preferred_element_type=f32).astype(bf16)
            gate_part = jnp.dot(rows[lead:], gate_full, preferred_element_type=f32).astype(bf16)
            up_part = lax.optimization_barrier(up_part)
            smoothed = conv_bias
            for k in range(3):
                back = lead - 2 + k
                smoothed = smoothed + conv_weight[k] * up_part[back : back + 2 * tok].astype(f32)
            hidden = (jax.nn.gelu(smoothed) * gate_part.astype(f32)).astype(bf16)
            part = jnp.dot(hidden, down_full, preferred_element_type=f32).astype(bf16)
            part = part.reshape(2, tok, width)
            theirs = lax.dynamic_index_in_dim(part, 1 - core, 0, keepdims=False)
            ours = lax.dynamic_index_in_dim(part, core, 0, keepdims=False)
            pair = ours.astype(f32) + hop_core(theirs).astype(f32)
            if dx:
                pair = pair.astype(bf16)
                pair, gate_tie = lax.optimization_barrier((pair, gate_tie))
                pair = hop_x(pair, dx)
                pair = pair.astype(f32)
            total = total + pair
        return total.astype(bf16)

    return body


def solution(mesh):
    coords = [getattr(d, "coords", None) for d in mesh.devices[:, 0]]
    n_fs, n_tp = mesh.shape["fs"], mesh.shape["tp"]
    ny = len({c[1] for c in coords}) if None not in coords else 1
    if n_fs % ny:
        ny = 1
    return jax.shard_map(
        make_body(n_fs, n_tp, ny),
        mesh=mesh,
        in_specs=(
            P(("fs", "tp"), None),
            P(("fs", "tp"), None),
            P(("fs", "tp"), None),
            P(),
            P("fs", "tp"),
            P("fs", "tp"),
            P(None, "tp"),
            P("tp"),
            P("tp", "fs"),
        ),
        out_specs=P(("fs", "tp"), None),
        check_vma=False,
    )
```

profile of v0, /device:TPU:0, one launch (start us, length us, event | category | flops | bytes accessed | tf_op | source)
XLA Modules:
  0.0 369.2 jit_solution(9452142283325952763)
XLA Ops:
  6.5 0.0 copy-start
  6.5 0.0 all-gather.2.cloned.1.call-start
  6.5 2.4 copy.15.refs_1_
  8.9 2.2 copy.16.refs_2_
  11.1 1.9 copy.14
  13.0 149.7 %shard_map.91 = (bf16[2048,2048]{1,0:T(8,128)(2,1)}, bf16[2048,1376]{1,0:T(8,128)(2,1)}, bf16[2048,1376]{1,0:T(8,128)(2,1)}) custom-call(bf16[64,2048]{1,0:T(8,128)(2,1)} %refs_0_.1, bf16[256,1376]{1,0:T(8,128)(2,1)} %copy.15.refs_1_, bf16[256,1376]{1,0:T(8,128)(2,1)} %copy.16.refs_2_), custom_call_target="tpu_custom_call" | custom-call | flops 99999997952 | bytes 10000000 | tf_op jit(solution)/shard_map/pallas_call | solution.py:195
  162.7 0.0 copy-done
  162.7 0.0 copy-start.4
  162.7 8.1 %fusion.22 = (f32[384]{0:T(512)S(1)}, bf16[384,2048]{0,1:T(8,128)(2,1)S(1)}) fusion(bf16[2048,2048]{1,0:T(8,128)(2,1)} %get-tuple-element.14, bf16[384,2048]{1,0:T(8,128)(2,1)S(1)} %copy-done, bf16[384,2048]{0,1:T(8,128)(2,1)S(1)} %copy.14), kind=kOutput, calls=%fused_computation.35 | convolution fusion | flops 3225943552 | bytes 13108736 | tf_op jit(solution)/shard_map/dot_general | solution.py:240
  170.8 0.0 copy-start.2
  170.8 0.0 copy-start.3
  170.8 1.1 copy-done.2
  171.9 0.0 copy-done.4
  171.9 1.6 fusion.24
  173.5 0.0 all-gather.2.cloned.1.call-update
  173.6 0.0 copy-done.3
  173.6 0.1 slice_reduce_fusion.2
  173.6 68.8 %shard_map.92 = bf16[1376,2048]{1,0:T(8,128)(2,1)} custom-call(bf16[1376,256]{1,0:T(8,128)(2,1)} %refs_0_.2), custom_call_target="tpu_custom_call" | custom-call | flops 99999997952 | bytes 10000000 | tf_op jit(solution)/shard_map/pallas_call | solution.py:195
  242.4 0.0 all-gather.2.cloned.1.call-done
  242.4 0.0 copy-start.5
  242.4 10.6 %fusion.21 = bf16[784,1376]{1,0:T(8,128)(2,1)} fusion(bf16[2048,1376]{1,0:T(8,128)(2,1)} %get-tuple-element.22, s32[]{:T(128)S(6)} %select_n.36, bf16[1536,2048]{0,1:T(8,128)(2,1)} %all-gather.2.cloned.1.call-done), kind=kOutput, calls=%fused_computation.30 | convolution fusion | flops 4419778048 | bytes 14085124 | tf_op jit(solution)/shard_map/dot_general | solution.py:258
  253.0 0.0 copy-done.5
  253.0 20.7 %convolution_convert_fusion.2 = bf16[768,2048]{1,0:T(8,128)(2,1)} fusion(bf16[1376,2048]{1,0:T(8,128)(2,1)} %shard_map.92, bf16[2048,1376]{1,0:T(8,128)(2,1)} %get-tuple-element.19, s32[]{:T(128)S(6)} %add.125, bf16[1536,2048]{0,1:T(8,128)(2,1)} %all-gather.2.cloned.1.call-done, bf16[784,1376]{1,0:T(8,128)(2,1)} %fusion.21, ...), kind=kOutput, calls=%fused_computation.33 | convolution fusion | flops 8680808448 | bytes 27350532 | tf_op jit(solution)/shard_map/dot_general | solution.py:266
  273.7 2.2 constant_dynamic-slice_fusion.3
  275.9 1.6 copy.18
  277.5 0.0 collective-permute-start
  277.5 1.1 copy.22
  278.6 2.7 collective-permute-done
  281.2 3.0 fusion.27
  284.2 10.8 %fusion.20 = bf16[784,1376]{1,0:T(8,128)(2,1)} fusion(bf16[2048,1376]{1,0:T(8,128)(2,1)} %get-tuple-element.22, s32[]{:T(128)S(6)} %select_n.41, bf16[1536,2048]{0,1:T(8,128)(2,1)} %all-gather.2.cloned.1.call-done), kind=kOutput, calls=%fused_computation.29 | convolution fusion | flops 4419778048 | bytes 14085124 | tf_op jit(solution)/shard_map/dot_general | solution.py:258
  295.0 21.2 %convolution_convert_fusion = bf16[768,2048]{1,0:T(8,128)(2,1)} fusion(bf16[1376,2048]{1,0:T(8,128)(2,1)} %shard_map.92, bf16[2048,1376]{1,0:T(8,128)(2,1)} %get-tuple-element.19, s32[]{:T(128)S(6)} %add.126, bf16[1536,2048]{0,1:T(8,128)(2,1)} %all-gather.2.cloned.1.call-done, bf16[784,1376]{1,0:T(8,128)(2,1)} %fusion.20, f32[1376]{0:T(1024)S(1)} %get-tuple-element.24, ...), kind=kOutput, calls=%fused_computation.31 | convolution fusion | flops 8680808448 | bytes 27350532 | tf_op jit(solution)/shard_map/dot_general | solution.py:266
  316.2 2.2 constant_dynamic-slice_fusion.1
  318.4 1.6 copy.20
  320.0 0.1 collective-permute-start.2
  320.1 0.1 collective-permute-start.1
  320.3 0.0 copy-start.1
  320.3 1.6 copy.23
  321.9 1.9 collective-permute-done.2
  323.7 33.4 %collective-permute-done.1 = bf16[384,2048]{0,1:T(8,128)(2,1)} collective-permute-done((bf16[384,2048]{0,1:T(8,128)(2,1)}, bf16[384,2048]{0,1:T(8,128)(2,1)}, u32[]{:S(2)}, u32[]{:S(2)}) %collective-permute-start.1) | collective-permute-done | bytes 1572896 | tf_op jit(solution)/shard_map/ppermute | solution.py:216
  357.1 3.6 fusion.26
  360.7 1.6 copy.21
  362.3 0.0 copy-done.1
  (1 shorter events, 0.0 us)
Async XLA Ops:
  6.5 156.1 %copy-start = (bf16[384,2048]{1,0:T(8,128)(2,1)S(1)}, bf16[384,2048]{1,0:T(8,128)(2,1)}, u32[]{:S(2)}) copy-start(bf16[384,2048]{1,0:T(8,128)(2,1)} %param.9) | copy-start | bytes 4718596
  6.5 235.9 %all-gather.2.cloned.1.call-start = ((), (), s32[]{:S(2)}) async-start(), calls=%async_computation | async-start | bytes 7864320 | tf_op jit(solution)/shard_map/all_gather | solution.py:249
  162.7 9.2 %copy-start.4 = (f32[2048]{0:T(1024)S(1)}, f32[2048]{0:T(1024)}, u32[]{:S(2)}) copy-start(f32[2048]{0:T(1024)} %param.12) | copy-start | bytes 24580
  170.8 1.1 copy-start.2
  170.8 2.8 copy-start.3
  242.4 10.6 %copy-start.5 = (f32[1376]{0:T(1024)S(1)}, f32[1376]{0:T(1024)}, u32[]{:S(2)}) copy-start(f32[1376]{0:T(1024)} %param.16) | copy-start | bytes 16516
  277.5 3.8 %collective-permute-start = (bf16[384,2048]{0,1:T(8,128)(2,1)}, bf16[384,2048]{0,1:T(8,128)(2,1)}, u32[]{:S(2)}, u32[]{:S(2)}) collective-permute-start(bf16[384,2048]{0,1:T(8,128)(2,1)} %bitcast.24), channel_id=1, source_target_pairs={{0,1},{1,0},{2,3},{3,2},{4,5},{5,4},{6,7},{7,6},{8,9},{9,8},{10,11... | collective-permute-start | bytes 4718600 | tf_op jit(solution)/shard_map/ppermute | solution.py:221
  320.0 3.8 %collective-permute-start.2 = (bf16[384,2048]{0,1:T(8,128)(2,1)}, bf16[384,2048]{0,1:T(8,128)(2,1)}, u32[]{:S(2)}, u32[]{:S(2)}) collective-permute-start(bf16[384,2048]{0,1:T(8,128)(2,1)} %bitcast.25), channel_id=1, source_target_pairs={{0,1},{1,0},{2,3},{3,2},{4,5},{5,4},{6,7},{7,6},{8,9},{9,8},{10,11... | collective-permute-start | bytes 4718600 | tf_op jit(solution)/shard_map/ppermute | solution.py:221
  320.1 37.0 %collective-permute-start.1 = (bf16[384,2048]{0,1:T(8,128)(2,1)}, bf16[384,2048]{0,1:T(8,128)(2,1)}, u32[]{:S(2)}, u32[]{:S(2)}) collective-permute-start(bf16[384,2048]{0,1:T(8,128)(2,1)} %fusion.27), channel_id=1, source_target_pairs={{0,2},{1,3},{2,0},{3,1},{4,6},{5,7},{6,4},{7,5},{8,10},{9,11},{10,... | collective-permute-start | bytes 4718600 | tf_op jit(solution)/shard_map/ppermute | solution.py:216
  320.3 42.1 %copy-start.1 = (bf16[384,2048]{1,0:T(8,128)(2,1)S(1)}, bf16[384,2048]{1,0:T(8,128)(2,1)}, u32[]{:S(2)}) copy-start(bf16[384,2048]{1,0:T(8,128)(2,1)} %param.9) | copy-start | bytes 4718596
Sparse Core Ops, SparseCore 0:
  173.6 47.4 all-gather.1
where the time goes:
time: 369 us
  Pallas kernels  218 us (59%)
  matrix products  71.3 us (19%)
  waiting for transfers between devices  37.9 us (10%)
  local copies, waits for them, and re-layouts  19.5 us (5%)
  between operations  13.6 us (4%)
  other arithmetic  8.17 us (2%)
    pallas_call x2, Pallas kernels, fs_gather(): pl.pallas_call(functools.partial(gather_kernel, nz, ny, nx, tuple(plan),...  218 us
    dot_general x2, matrix products, body(): part = jnp.dot(hidden, down_full, preferred_element_type=f32).astype(bf16)  41.9 us
    ppermute x1, waiting for transfers between devices, hop_x(): lax.ppermute(a, 'tp', [(x * 2 + c, (x + dx) % nx * 2 + c) for x in range(...  33.4 us
    dot_general x2, matrix products, body(): up_part = jnp.dot(rows, gate_tie, preferred_element_type=f32).astype(bf16)  21.3 us
    unnamed x17, local copies, waits for them, and re-layouts  10.2 us
    dot_general x1, matrix products, body(): summed = jnp.dot(mixed, mix_full, preferred_element_type=f32)  8.07 us
  transfers between devices with their start and end apart: 4, of which 3 were waited for; matrix products, arithmetic and copies ran while one was open for 1% of the time, Pallas kernels for 19%

commit v1 on v0

--- a/solution.py
+++ b/solution.py
@@ -13,7 +13,7 @@
 MESH = pl.DeviceIdType.MESH
 
 
-def gather_kernel(nz, ny, nx, plan, count, spread, *refs):
+def gather_kernel(nz, ny, nx, plan, count, spread, share, *refs):
     shards, fulls = refs[:count], refs[count : 2 * count]
     send_sem, recv_sem, local_sem, tp_send, tp_recv = refs[2 * count :]
     n_fs = nz * ny
@@ -95,6 +95,23 @@
                 tp_copy(f, x_at(dx), 0, x_at(dx)).wait_recv()
             act(tp_copy(f, x_at(dx), nx - 1 + dx, tp + 1 - 2 * core))
 
+    def shared(t):
+        rows = shards[-1].shape[0]
+        return fulls[-1].at[pl.ds(pl.multiple_of(t * rows, 16), rows), :]
+
+    def share_copy(t, lane, to, mine=False):
+        return pltpu.make_async_remote_copy(
+            src_ref=shards[-1] if mine else shared(t),
+            dst_ref=shared(t),
+            send_sem=tp_send.at[0, lane],
+            recv_sem=tp_recv.at[0, t],
+            device_id={"tp": to},
+            device_id_type=MESH,
+        )
+
+    def share_local():
+        return pltpu.make_async_copy(shards[-1], shared(tp), local_sem.at[len(plan)])
+
     def local(c):
         return pltpu.make_async_copy(own(c), piece(c, me), local_sem.at[c])
 
@@ -103,12 +120,19 @@
     greet += [fs_at(z, dy) for dy in range(1, ny)]
     for other in greet:
         pl.semaphore_signal(barrier, inc=1, device_id={"fs": other}, device_id_type=MESH)
-    greet_tp = [x_at(dx) for dx in range(1, nx)] + [tp + 1 - 2 * core] if spread else []
+    greet_tp = [x_at(dx) for dx in range(1, nx)] + [tp + 1 - 2 * core]
+    greet_tp = greet_tp if spread or share else []
     for other in greet_tp:
         pl.semaphore_signal(barrier, inc=1, device_id={"tp": other}, device_id_type=MESH)
     pl.semaphore_wait(barrier, len(greet) + len(greet_tp))
 
     def walk(act, wait):
+        if share:
+            for dx in range(1, nx):
+                act(share_copy(tp, dx - 1, x_at(dx), True))
+            act(share_copy(tp, nx - 1, tp + 1 - 2 * core, True))
+            if wait:
+                share_local().start()
         for c in range(len(plan)):
             y_sends(act, c, me, True)
             z_sends(act, c, me, True, True, True)
@@ -158,12 +182,22 @@
                             if spread and c == 0:
                                 tp_sends(act, f)
 
+        if share:
+            for dx in range(1, nx):
+                if wait:
+                    share_copy(x_at(dx), 0, x_at(dx)).wait_recv()
+                act(share_copy(x_at(dx), nx - 1 + dx, tp + 1 - 2 * core))
         if spread:
             both(nz - 1, from_y)
             for f in range(n_fs):
                 tp_relay(act, f, wait)
 
     walk(lambda d: d.start(), True)
+    if share:
+        for dx in range(nx):
+            t = x_at(dx) + 1 - 2 * core
+            share_copy(t, 0, tp + 1 - 2 * core).wait_recv()
+        share_local().wait()
     if spread:
         for f in range(n_fs):
             for dx in range(nx):
@@ -179,7 +213,7 @@
     walk(lambda d: d.wait_send(), False)
 
 
-def fs_gather(shards, axes, chunks, y_first, nz, ny, nx, spread, ident):
+def fs_gather(shards, axes, chunks, y_first, nz, ny, nx, spread, ident, rows=None):
     n_fs = nz * ny
     plan, shapes = [], []
     for m, (w, axis) in enumerate(zip(shards, axes)):
@@ -191,16 +225,19 @@
         shape = list(w.shape)
         shape[axis] = block * n_fs * (2 * nx if spread and m == 0 else 1)
         shapes.append(jax.ShapeDtypeStruct(tuple(shape), w.dtype))
+    if rows is not None:
+        shards = (*shards, rows)
+        shapes.append(jax.ShapeDtypeStruct((rows.shape[0] * 2 * nx, rows.shape[1]), rows.dtype))
     n = len(plan)
     return pl.pallas_call(
-        functools.partial(gather_kernel, nz, ny, nx, tuple(plan), len(shards), spread),
+        functools.partial(gather_kernel, nz, ny, nx, tuple(plan), len(shards), spread, rows is not None),
         out_shape=shapes,
         in_specs=[pl.BlockSpec(memory_space=pl.ANY)] * len(shards),
         out_specs=[pl.BlockSpec(memory_space=pl.ANY)] * len(shards),
         scratch_shapes=[
             pltpu.SemaphoreType.DMA((1 + ny, n_fs, n)),
             pltpu.SemaphoreType.DMA((n_fs, n)),
-            pltpu.SemaphoreType.DMA((n,)),
+            pltpu.SemaphoreType.DMA((n + 1,)),
             pltpu.SemaphoreType.DMA((n_fs, 2 * nx - 1)),
             pltpu.SemaphoreType.DMA((n_fs, 2 * nx)),
         ],
@@ -245,10 +282,9 @@
             * lax.rsqrt(jnp.mean(x_float * x_float, axis=-1, keepdims=True) + norm_eps)
             * norm_gain
         ).astype(bf16)
-        normed, down_weight = lax.optimization_barrier((normed, down_weight))
-        tokens = lax.all_gather(normed, "tp", axis=0, tiled=True)
-        (down_full,) = fs_gather((down_weight,), (1,), 2, (), nz, ny, nx, False, 1)
-        tokens, down_full = lax.optimization_barrier((tokens, down_full))
+        down_full, tokens = fs_gather(
+            (down_weight,), (1,), 2, (), nz, ny, nx, False, 1, normed
+        )
         lead = 16
         tokens = jnp.pad(tokens, ((lead, 0), (0, 0)))
         total, gate_tie = x_float, up_full

time: 369 us -> 349 us (0.946)
  between operations: 13.6 us -> 0.12 us
  local copies, waits for them, and re-layouts: 19.5 us -> 8.92 us
  Pallas kernels: 218 us -> 225 us
  matrix products: 71.3 us -> 65.3 us
    dynamic_slice x4 -> x0, local copies, waits for them, and re-layouts: 7.55 us -> none  [the longest x2 4.39 us: body(): ours = lax.dynamic_index_in_dim(part, core, 0, keepdims=False)]
    pallas_call x2, Pallas kernels: 218 us -> 225 us  [fs_gather(): pl.pallas_call(functools.partial(gather_kernel, nz, ny, nx, tuple(plan),...]
    unnamed x17 -> x14, local copies, waits for them, and re-layouts: 10.2 us -> 4.63 us
    squeeze x0 -> x2, local copies, waits for them, and re-layouts: none -> 4.24 us  [body(): theirs = lax.dynamic_index_in_dim(part, 1 - core, 0, keepdims=False)]
  transfers between devices with their start and end apart: 4 -> 3, of which waited for: 3 -> 3; matrix products, arithmetic and copies ran while one was open for 1% -> 0% of each run, Pallas kernels for 19% -> 0%
where the time goes in v1:
time: 349 us; the launch traced here: 348 us
  Pallas kernels  225 us (64%)
  matrix products  65.3 us (19%)
  waiting for transfers between devices  39.3 us (11%)
  local copies, waits for them, and re-layouts  8.92 us (3%)
  other arithmetic  8.54 us (2%)
    pallas_call x2, Pallas kernels, fs_gather(): pl.pallas_call(functools.partial(gather_kernel, nz, ny, nx, tuple(plan),...  225 us
    dot_general x2, matrix products, body(): part = jnp.dot(hidden, down_full, preferred_element_type=f32).astype(bf16)  38.8 us
    ppermute x1, waiting for transfers between devices, hop_x(): lax.ppermute(a, 'tp', [(x * 2 + c, (x + dx) % nx * 2 + c) for x in range(...  33.6 us
    dot_general x2, matrix products, body(): up_part = jnp.dot(rows, gate_tie, preferred_element_type=f32).astype(bf16)  19 us
    dot_general x1, matrix products, body(): summed = jnp.dot(mixed, mix_full, preferred_element_type=f32)  7.45 us
  transfers between devices with their start and end apart: 3, of which 3 were waited for; matrix products, arithmetic and copies ran while one was open for 0% of the time, Pallas kernels for 0%

profile of v1, /device:TPU:0, one launch (start us, length us, event | category | flops | bytes accessed | tf_op | source)
XLA Modules:
  0.0 348.4 jit_solution(3369784919359669901)
XLA Ops:
  0.0 0.0 copy-start
  0.0 2.4 copy.10.refs_1_
  2.4 2.2 copy.11.refs_2_
  4.6 149.6 %shard_map.91 = (bf16[2048,2048]{1,0:T(8,128)(2,1)}, bf16[2048,1376]{1,0:T(8,128)(2,1)}, bf16[2048,1376]{1,0:T(8,128)(2,1)}) custom-call(bf16[64,2048]{1,0:T(8,128)(2,1)} %refs_0_.2, bf16[256,1376]{1,0:T(8,128)(2,1)} %copy.10.refs_1_, bf16[256,1376]{1,0:T(8,128)(2,1)} %copy.11.refs_2_), custom_call_target="tpu_custom_call" | custom-call | flops 99999997952 | bytes 10000000 | tf_op jit(solution)/shard_map/pallas_call | solution.py:232
  154.2 0.0 copy-done
  154.3 0.0 copy-start.4
  154.3 7.4 %fusion.18 = (f32[384]{0:T(512)S(1)}, bf16[384,2048]{1,0:T(8,128)(2,1)S(1)}) fusion(bf16[384,2048]{1,0:T(8,128)(2,1)S(1)} %copy-done, bf16[2048,2048]{1,0:T(8,128)(2,1)} %get-tuple-element.12, bf16[384,2048]{1,0:T(8,128)(2,1)} %param.10), kind=kOutput, calls=%fused_computation.33 | convolution fusion | flops 3225943552 | bytes 13108736 | tf_op jit(solution)/shard_map/dot_general | solution.py:277
  161.7 0.0 copy-start.1
  161.7 0.0 copy-done.4
  161.8 1.6 fusion.20.refs_1_
  163.4 75.1 %shard_map.92 = (bf16[1376,2048]{1,0:T(8,128)(2,1)}, bf16[1536,2048]{1,0:T(8,128)(2,1)}) custom-call(bf16[1376,256]{1,0:T(8,128)(2,1)} %refs_0_.3, bf16[384,2048]{1,0:T(8,128)(2,1)} %fusion.20.refs_1_), custom_call_target="tpu_custom_call" | custom-call | flops 99999997952 | bytes 10000000 | tf_op jit(solution)/shard_map/pallas_call | solution.py:232
  238.5 0.0 copy-done.1
  238.5 0.0 copy-start.3
  238.6 0.0 copy-start.5
  238.6 9.6 %convolution_convert_fusion.1 = bf16[784,1376]{1,0:T(8,128)(2,1)} fusion(bf16[2048,1376]{1,0:T(8,128)(2,1)} %get-tuple-element.18, s32[]{:T(128)S(6)} %select_n.36, bf16[1536,2048]{1,0:T(8,128)(2,1)} %get-tuple-element.13), kind=kOutput, calls=%fused_computation.28 | convolution fusion | flops 4419778048 | bytes 14085124 | tf_op jit(solution)/shard_map/dot_general | solution.py:294
  248.1 0.0 copy-done.3
  248.2 0.0 copy-done.5
  248.2 19.1 %convolution_convert_fusion.4 = bf16[768,2048]{1,0:T(8,128)(2,1)} fusion(bf16[1376,2048]{1,0:T(8,128)(2,1)} %get-tuple-element.16, bf16[2048,1376]{1,0:T(8,128)(2,1)} %get-tuple-element.15, s32[]{:T(128)S(6)} %add.125, bf16[1536,2048]{1,0:T(8,128)(2,1)} %get-tuple-element.13, bf16[784,1376]{1,0:T(8,128)(2,1)} %convolution_convert_fusion.1, ...), kind=kOutput, calls=%fused_computation.31 | convolution fusion | flops 8680808448 | bytes 27350532 | tf_op jit(solution)/shard_map/dot_general | solution.py:302
  267.3 2.7 dynamic-slice_bitcast_fusion.1
  270.0 0.2 collective-permute-start
  270.3 3.4 collective-permute-done
  273.6 3.2 fusion.23
  276.8 9.4 %convolution_convert_fusion = bf16[784,1376]{1,0:T(8,128)(2,1)} fusion(bf16[2048,1376]{1,0:T(8,128)(2,1)} %get-tuple-element.18, s32[]{:T(128)S(6)} %select_n.41, bf16[1536,2048]{1,0:T(8,128)(2,1)} %get-tuple-element.13), kind=kOutput, calls=%fused_computation.27 | convolution fusion | flops 4419778048 | bytes 14085124 | tf_op jit(solution)/shard_map/dot_general | solution.py:294
  286.2 0.0 copy-start.2
  286.2 19.8 %convolution_convert_fusion.2 = bf16[768,2048]{1,0:T(8,128)(2,1)} fusion(bf16[1376,2048]{1,0:T(8,128)(2,1)} %get-tuple-element.16, bf16[2048,1376]{1,0:T(8,128)(2,1)} %get-tuple-element.15, s32[]{:T(128)S(6)} %add.126, bf16[1536,2048]{1,0:T(8,128)(2,1)} %get-tuple-element.13, bf16[784,1376]{1,0:T(8,128)(2,1)} %convolution_convert_fusion, ...), kind=kOutput, calls=%fused_computation.29 | convolution fusion | flops 8680808448 | bytes 27350532 | tf_op jit(solution)/shard_map/dot_general | solution.py:302
  306.0 1.5 dynamic-slice_bitcast_fusion
  307.5 0.3 collective-permute-start.2
  307.8 0.8 collective-permute-start.1
  308.7 2.3 collective-permute-done.2
  311.0 33.6 %collective-permute-done.1 = bf16[384,2048]{1,0:T(8,128)(2,1)S(1)} collective-permute-done((bf16[384,2048]{1,0:T(8,128)(2,1)}, bf16[384,2048]{1,0:T(8,128)(2,1)S(1)}, u32[]{:S(2)}, u32[]{:S(2)}) %collective-permute-start.1) | collective-permute-done | bytes 1572896 | tf_op jit(solution)/shard_map/ppermute | solution.py:253
  344.6 0.0 copy-done.2
  344.6 3.8 %fusion.22 = bf16[384,2048]{1,0:T(8,128)(2,1)} fusion(bf16[384,2048]{1,0:T(8,128)(2,1)S(1)} %copy-done.2, bf16[384,2048]{1,0:T(8,128)(2,1)S(1)} %collective-permute-done.2, bf16[384,2048]{1,0:T(8,128)(2,1)S(1)} %collective-permute-done.1, bf16[2,384,2048]{2,1,0:T(8,128)(2,1)} %bitcast.27, s32[]{:T(128)S(6)} %select_n.38), kind=kLoop, calls=%fused_computation.37 | loop fusion | flops 6291456 | bytes 7864324 | tf_op jit(solution)/shard_map/convert_element_type | solution.py:313
  (2 shorter events, 0.1 us)
Async XLA Ops:
  0.0 154.2 %copy-start = (bf16[384,2048]{1,0:T(8,128)(2,1)S(1)}, bf16[384,2048]{1,0:T(8,128)(2,1)}, u32[]{:S(2)}) copy-start(bf16[384,2048]{1,0:T(8,128)(2,1)} %param.9) | copy-start | bytes 4718596
  154.3 7.5 %copy-start.4 = (f32[2048]{0:T(1024)S(1)}, f32[2048]{0:T(1024)}, u32[]{:S(2)}) copy-start(f32[2048]{0:T(1024)} %param.12) | copy-start | bytes 24580
  161.7 76.8 %copy-start.1 = (bf16[384,2048]{1,0:T(8,128)(2,1)}, bf16[384,2048]{1,0:T(8,128)(2,1)S(1)}, u32[]{:S(2)}) copy-start(bf16[384,2048]{1,0:T(8,128)(2,1)S(1)} %get-tuple-element.23) | copy-start | bytes 4718596
  238.5 9.6 %copy-start.3 = (f32[3,1376]{1,0:T(4,128)S(1)}, f32[3,1376]{1,0:T(4,128)}, u32[]{:S(2)}) copy-start(f32[3,1376]{1,0:T(4,128)} %param.15) | copy-start | bytes 49540
  238.6 9.6 %copy-start.5 = (f32[1376]{0:T(1024)S(1)}, f32[1376]{0:T(1024)}, u32[]{:S(2)}) copy-start(f32[1376]{0:T(1024)} %param.16) | copy-start | bytes 16516
  270.0 3.6 %collective-permute-start = (bf16[384,2048]{1,0:T(8,128)(2,1)}, bf16[384,2048]{1,0:T(8,128)(2,1)S(1)}, u32[]{:S(2)}, u32[]{:S(2)}) collective-permute-start(bf16[384,2048]{1,0:T(8,128)(2,1)} %dynamic-slice_bitcast_fusion.1), channel_id=1, source_target_pairs={{0,1},{1,0},{2,3},{3,2},{4,5},{5,4},{6,7},{7,6},{8,9},{9,8},{10,11... | collective-permute-start | bytes 4718600 | tf_op jit(solution)/shard_map/ppermute | solution.py:258
  286.2 58.4 %copy-start.2 = (bf16[384,2048]{1,0:T(8,128)(2,1)S(1)}, bf16[384,2048]{1,0:T(8,128)(2,1)}, u32[]{:S(2)}) copy-start(bf16[384,2048]{1,0:T(8,128)(2,1)} %copy-done.1) | copy-start | bytes 4718596
  307.5 3.5 collective-permute-start.2
  307.8 36.8 %collective-permute-start.1 = (bf16[384,2048]{1,0:T(8,128)(2,1)}, bf16[384,2048]{1,0:T(8,128)(2,1)S(1)}, u32[]{:S(2)}, u32[]{:S(2)}) collective-permute-start(bf16[384,2048]{1,0:T(8,128)(2,1)} %fusion.23), channel_id=1, source_target_pairs={{0,2},{1,3},{2,0},{3,1},{4,6},{5,7},{6,4},{7,5},{8,10},{9,11},{10,... | collective-permute-start | bytes 4718600 | tf_op jit(solution)/shard_map/ppermute | solution.py:253
